TPU v7x, 32 devices: a whole 2x2x4 slice. The times are simulated.
32 devices in a mesh: ep: 8 (over z, y), tp: 4 (over x, core).
Axes of the slice: x: 2, y: 2, z: 4, core: 2. Of those that a mesh axis runs over, the one named last changes fastest.
Arguments:
- tokens: bfloat16 [1024, 2048], P('ep'), may hold values from -6 to 6
- norm_gain: float32 [2048], replicated, may hold values from 0.1 to 1.9
- routes: int32 [1024, 2], P('ep'), may hold values from 0 to 7, all different within a row; in each aligned block of 128 rows (0 to 127, 128 to 255, ...) at most 48 rows name the same one
- group_prob: float32 [1024], P('ep'), may hold values from 0.2 to 1
- expert_logits: float32 [1024, 2], P('ep'), may hold values from -6 to 6
- gate_weight: bfloat16 [8, 2048, 384], P('ep', None, 'tp'), may hold values from -0.125 to 0.125
- up_weight: bfloat16 [8, 2048, 384], P('ep', None, 'tp'), may hold values from -0.125 to 0.125
- down_matrix: bfloat16 [8, 384, 2048], P('ep', 'tp'), may hold values from -0.3125 to 0.3125
Outputs:
- combined: bfloat16 [1024, 2048], P('ep', 'tp')
Inputs may be any that keep to these rules, and one draw needn't show every extreme that they name: `routes`: each row names 2 different experts. Among the 128 tokens of one index of ep at most 48 rows name one expert, and in every draw some expert is named by exactly 48 of them.
All inputs are finite; a program needn't handle non-finite values.
Results may differ from a plain program's by a relative error of at most 0.013.
Values may be sent and summed in bfloat16 or wider, within the bound.
A program may use at most 64 MiB of HBM per device.

v0:
```python
import jax
import jax.numpy as jnp
from jax import lax
from jax.sharding import PartitionSpec as P


def hidden_part(buffer, gate_weight, up_weight):
    local_count = gate_weight.shape[0]
    grouped = buffer.reshape(
        buffer.shape[0] // local_count, local_count, buffer.shape[1], buffer.shape[2]
    )
    gate_proj = jnp.einsum(
        "sknd,kdf->sknf", grouped, gate_weight, preferred_element_type=jnp.float32
    )
    up_proj = jnp.einsum("sknd,kdf->sknf", grouped, up_weight, preferred_element_type=jnp.float32)
    hidden_state = (jax.nn.silu(gate_proj) * up_proj).astype(jnp.bfloat16)
    return hidden_state.reshape(buffer.shape[0], buffer.shape[1], hidden_state.shape[3])


def down_blocks(hidden_full, down_cols, block_count):
    local_count = down_cols.shape[0]
    width = hidden_full.shape[2] // block_count
    grouped = hidden_full.reshape(
        hidden_full.shape[0] // local_count, local_count, hidden_full.shape[1], block_count, width
    )
    columns = down_cols.reshape(local_count, block_count, width, down_cols.shape[2])
    block_list = jnp.einsum(
        "sknrf,krfd->sknrd", grouped, columns, preferred_element_type=jnp.float32
    ).astype(jnp.bfloat16)
    summed = jnp.sum(block_list.astype(jnp.float32), 3).astype(jnp.bfloat16)
    return summed.reshape(hidden_full.shape[0], hidden_full.shape[1], down_cols.shape[2])


def body(tokens, norm_gain, routes, group_prob, expert_logits, gate_weight, up_weight, down_matrix):
    tok_rows, model_width = tokens.shape
    top_count = routes.shape[1]
    experts = gate_weight.shape[0] * lax.axis_size("ep")
    capacity = 3 * top_count * tok_rows // (2 * experts)
    block_count = lax.axis_size("tp")
    down_cols = lax.all_to_all(down_matrix, "tp", split_axis=2, concat_axis=1, tiled=True)
    values = tokens.astype(jnp.float32)
    normed = (
        values * lax.rsqrt(jnp.mean(values * values, -1, keepdims=True) + 1e-06) * norm_gain
    ).astype(jnp.bfloat16)
    flat_ids = routes.reshape(-1)
    onehot = (flat_ids[:, None] == jnp.arange(experts, dtype=jnp.int32)[None, :]).astype(jnp.int32)
    earlier = jnp.cumsum(onehot, 0) - onehot
    slot_index = jnp.sum(earlier * onehot, 1)
    target = flat_ids * capacity + slot_index
    owners = jnp.arange(tok_rows * top_count, dtype=jnp.int32) // top_count
    outgoing = (
        jnp.zeros((experts * capacity, model_width), jnp.bfloat16).at[target].set(normed[owners])
    )
    outgoing = outgoing.reshape(experts, capacity, model_width)
    hidden_state = hidden_part(
        lax.all_to_all(outgoing, "ep", split_axis=0, concat_axis=0, tiled=True),
        gate_weight,
        up_weight,
    )
    hidden_full = lax.all_gather(hidden_state, "tp", axis=2, tiled=True)
    summed = down_blocks(hidden_full, down_cols, block_count)
    returned = lax.all_to_all(summed, "ep", split_axis=0, concat_axis=0, tiled=True)
    flat_back = returned.reshape(experts * capacity, returned.shape[2])
    weights = group_prob[:, None] * jax.nn.softmax(expert_logits, axis=-1)
    picked = flat_back[target].reshape(tok_rows, top_count, flat_back.shape[1]).astype(jnp.float32)
    combined = jnp.sum(picked * weights[:, :, None], 1).astype(jnp.bfloat16)
    return combined


def solution(mesh):
    return jax.shard_map(
        body,
        mesh=mesh,
        in_specs=(
            P("ep", None),
            P(),
            P("ep", None),
            P("ep"),
            P("ep", None),
            P("ep", None, "tp"),
            P("ep", None, "tp"),
            P("ep", "tp", None),
        ),
        out_specs=P("ep", "tp"),
        check_vma=False,
    )
```

profile of v0, /device:TPU:0, one launch (start us, length us, event | category | flops | bytes accessed | tf_op | source)
XLA Modules:
  0.0 104.3 jit_solution(11414660805682031129)
XLA Ops:
  0.0 0.0 copy-start
  0.0 2.4 %copy.32 = bf16[1,96,2048]{1,0,2:T(2,128)(2,1)S(1)} copy(bf16[1,96,2048]{2,1,0:T(8,128)(2,1)} %param.15) | data formatting | bytes 786432 | tf_op args[7]
  2.4 0.5 broadcast.137
  2.9 11.6 %reduce.6 = bf16[2048,96]{1,0:T(8,128)(2,1)S(1)} reduce(bf16[2048,1,96]{2,1,0:T(2,128)(2,1)S(1)} %bitcast.53, bf16[]{:T(256)} %broadcast.137), dimensions={1}, to_apply=%bitcast.44.reduce_sub_computation | reduce | bytes 786434
  14.5 0.0 copy-start.3
  14.5 1.6 %reshape.188 = bf16[4,2,24576]{2,1,0:T(2,128)(2,1)} reshape(bf16[2048,96]{1,0:T(8,128)(2,1)S(1)} %reduce.6) | data formatting | bytes 786432
  16.1 4.2 %all-to-all-start = ((bf16[4,2,24576]{2,1,0:T(2,128)(2,1)}), bf16[4,2,24576]{2,1,0:T(2,128)(2,1)S(1)}, u32[]{:S(2)}, u32[]{:S(2)}) async-start(bf16[4,2,24576]{2,1,0:T(2,128)(2,1)} %reshape.188), calls=%async_computation | async-start | bytes 786432 | tf_op jit(solution)/shard_map/all_to_all | solution.py:40
  20.3 0.0 copy-done.4
  20.3 0.1 copy.38
  20.4 0.1 eq.29
  20.6 0.1 eq.25
  20.7 0.6 reduce-window.6
  21.3 0.2 slice_reduce_fusion
  21.6 0.1 copy.37
  21.7 0.1 mul.63
  21.9 0.0 copy-done.1
  21.9 0.2 fusion.2
  22.1 0.1 fusion.11
  22.1 0.0 copy-done.3
  22.2 0.2 fusion.4
  22.4 6.7 %scatter_custom_fusion = bf16[384,2048]{1,0:T(8,128)(2,1)} fusion(s32[256]{0:T(256)S(1)} %bitcast.57, bf16[128,2048]{1,0:T(8,128)(2,1)S(1)} %fusion.4, s32[1024]{0:T(1024)S(1)} %pad_clamp_fusion.1, bf16[]{:T(256)} %constant.32.clone.1), kind=kCustom, calls=%fused_computation.13 | custom fusion | bytes 1572866 | tf_op jit(solution)/shard_map/scatter | solution.py:52
  29.1 0.0 all-to-all-done
  29.1 6.7 %all-to-all-start.1 = ((bf16[8,48,2048]{2,1,0:T(8,128)(2,1)}), bf16[8,48,2048]{2,1,0:T(8,128)(2,1)S(1)}, u32[]{:S(2)}, u32[]{:S(2)}) async-start(bf16[8,48,2048]{2,1,0:T(8,128)(2,1)} %bitcast.6), calls=%async_computation.1 | async-start | bytes 3145728 | tf_op jit(solution)/shard_map/all_to_all | solution.py:56
  35.9 0.8 reshape.189
  36.6 1.9 %fusion.14 = (bf16[1,96,512]{1,0,2:T(2,128)(2,1)}, bf16[1,96,512]{1,0,2:T(2,128)(2,1)S(1)}, bf16[1,96,512]{1,0,2:T(2,128)(2,1)S(1)}, bf16[1,96,512]{1,0,2:T(2,128)(2,1)}) fusion(bf16[1,96,2048]{1,0,2:T(2,128)(2,1)S(1)} %bitcast.52), kind=kLoop, calls=%fused_computation.40 | loop fusion | bytes 786432 | tf_op jit(solution)/shard_map/slice.2
  38.5 1.1 %copy.33 = bf16[1,96,512]{2,1,0:T(8,128)(2,1)S(1)} copy(bf16[1,96,512]{1,0,2:T(2,128)(2,1)} %get-tuple-element.5) | data formatting | bytes 196608 | tf_op jit(solution)/shard_map/slice.2
  39.6 1.1 %copy.34 = bf16[1,96,512]{2,1,0:T(8,128)(2,1)S(1)} copy(bf16[1,96,512]{1,0,2:T(2,128)(2,1)} %get-tuple-element.8) | data formatting | bytes 196608 | tf_op jit(solution)/shard_map/slice.3
  40.7 0.1 copy.35
  40.8 0.1 copy.36
  40.9 0.0 copy-start.6
  41.0 32.3 %all-to-all-done.1 = bf16[8,48,2048]{2,1,0:T(8,128)(2,1)S(1)} async-done(((bf16[8,48,2048]{2,1,0:T(8,128)(2,1)}), bf16[8,48,2048]{2,1,0:T(8,128)(2,1)S(1)}, u32[]{:S(2)}, u32[]{:S(2)}) %all-to-all-start.1) | async-done | bytes 1572896 | tf_op jit(solution)/shard_map/all_to_all | solution.py:56
  73.3 0.0 copy-done
  73.3 0.6 convolution_bitcast_fusion.1
  73.9 0.0 copy-done.6
  73.9 0.6 fusion.1
  74.5 0.2 copy.40
  74.6 8.7 %all-gather = bf16[8,1,48,384]{2,0,1,3:T(8,128)(2,1)S(1)} all-gather(bf16[8,1,48,96]{2,0,1,3:T(8,128)(2,1)S(1)} %copy.40), channel_id=2, replica_groups=mesh['ep'=8,'tp'=4] {'tp'}, dimensions={3}, use_global_device_ids=true | all-gather | bytes 368640 | tf_op jit(solution)/shard_map/all_gather | solution.py:60
  83.4 0.5 copy.42
  83.9 0.5 fusion.15
  84.4 0.0 copy-start.2
  84.4 0.0 copy-start.5
  84.4 1.1 %convert_reduce_fusion = bf16[512,8,48]{0,2,1:T(8,128)(2,1)} fusion(f32[4,512,8,48]{1,3,2,0:T(8,128)S(1)} %bitcast.51), kind=kLoop, calls=%fused_computation.3 | loop fusion | flops 1376256 | bytes 3538944 | tf_op jit(solution)/shard_map/reduce_sum | solution.py:30
  85.6 3.6 %all-to-all-start.2 = ((bf16[8,48,512]{2,1,0:T(8,128)(2,1)}), bf16[8,48,512]{2,1,0:T(8,128)(2,1)S(1)}, u32[]{:S(2)}, u32[]{:S(2)}) async-start(bf16[8,48,512]{2,1,0:T(8,128)(2,1)} %bitcast.23), calls=%async_computation.2 | async-start | bytes 786432 | tf_op jit(solution)/shard_map/all_to_all | solution.py:62
  89.3 0.1 copy.43
  89.4 12.0 %all-to-all-done.2 = bf16[8,48,512]{2,1,0:T(8,128)(2,1)S(1)} async-done(((bf16[8,48,512]{2,1,0:T(8,128)(2,1)}), bf16[8,48,512]{2,1,0:T(8,128)(2,1)S(1)}, u32[]{:S(2)}, u32[]{:S(2)}) %all-to-all-start.2) | async-done | bytes 393248 | tf_op jit(solution)/shard_map/all_to_all | solution.py:62
  101.4 1.2 %gather_fusion = bf16[256,512]{1,0:T(8,128)(2,1)S(1)} fusion(bf16[384,512]{1,0:T(8,128)(2,1)S(1)} %bitcast.50, s32[1024]{0:T(1024)S(1)} %pad_clamp_fusion), kind=kCustom, calls=%fused_computation.1 | custom fusion | bytes 525312 | tf_op jit(solution)/shard_map/gather | solution.py:65
  102.6 0.3 reshape.150
  102.9 1.4 %multiply_reduce_fusion = bf16[128,512]{1,0:T(8,128)(2,1)} fusion(f32[128,2,512]{2,1,0:T(2,128)S(1)} %reshape.150, f32[128,2]{1,0:T(8,128)S(1)} %copy.43), kind=kLoop, calls=%fused_computation.16 | loop fusion | flops 196608 | bytes 656384 | tf_op jit(solution)/shard_map/reduce_sum | solution.py:66
  (17 shorter events, 0.2 us)
Async XLA Ops:
  0.0 73.3 %copy-start = (bf16[1,2048,96]{1,2,0:T(8,128)(2,1)S(1)}, bf16[1,2048,96]{1,2,0:T(8,128)(2,1)}, u32[]{:S(2)}) copy-start(bf16[1,2048,96]{1,2,0:T(8,128)(2,1)} %param.13) | copy-start | bytes 1179652
  2.9 17.4 %copy-start.4 = (s32[128,2]{0,1:T(2,128)S(1)}, s32[128,2]{0,1:T(2,128)}, u32[]{:S(2)}) copy-start(s32[128,2]{0,1:T(2,128)} %param.10) | copy-start | bytes 3076
  2.9 19.0 %copy-start.1 = (bf16[128,2048]{1,0:T(8,128)(2,1)S(1)}, bf16[128,2048]{1,0:T(8,128)(2,1)}, u32[]{:S(2)}) copy-start(bf16[128,2048]{1,0:T(8,128)(2,1)} %param.8) | copy-start | bytes 1572868
  14.5 7.6 %copy-start.3 = (f32[2048]{0:T(1024)S(1)}, f32[2048]{0:T(1024)}, u32[]{:S(2)}) copy-start(f32[2048]{0:T(1024)} %param.9) | copy-start | bytes 24580
  16.1 13.1 %all-to-all-start = ((bf16[4,2,24576]{2,1,0:T(2,128)(2,1)}), bf16[4,2,24576]{2,1,0:T(2,128)(2,1)S(1)}, u32[]{:S(2)}, u32[]{:S(2)}) async-start(bf16[4,2,24576]{2,1,0:T(2,128)(2,1)} %reshape.188), calls=%async_computation | async-start | bytes 786432 | tf_op jit(solution)/shard_map/all_to_all | solution.py:40
  29.1 44.2 %all-to-all-start.1 = ((bf16[8,48,2048]{2,1,0:T(8,128)(2,1)}), bf16[8,48,2048]{2,1,0:T(8,128)(2,1)S(1)}, u32[]{:S(2)}, u32[]{:S(2)}) async-start(bf16[8,48,2048]{2,1,0:T(8,128)(2,1)} %bitcast.6), calls=%async_computation.1 | async-start | bytes 3145728 | tf_op jit(solution)/shard_map/all_to_all | solution.py:56
  40.9 33.0 %copy-start.6 = (bf16[1,2048,96]{1,2,0:T(8,128)(2,1)S(1)}, bf16[1,2048,96]{1,2,0:T(8,128)(2,1)}, u32[]{:S(2)}) copy-start(bf16[1,2048,96]{1,2,0:T(8,128)(2,1)} %param.14) | copy-start | bytes 1179652
  84.4 4.8 %copy-start.2 = (f32[128,2]{0,1:T(2,128)S(1)}, f32[128,2]{0,1:T(2,128)}, u32[]{:S(2)}) copy-start(f32[128,2]{0,1:T(2,128)} %param.12) | copy-start | bytes 3076
  84.4 4.8 %copy-start.5 = (f32[128]{0:T(128)S(1)}, f32[128]{0:T(128)}, u32[]{:S(2)}) copy-start(f32[128]{0:T(128)} %param.11) | copy-start | bytes 1540
  85.6 15.9 %all-to-all-start.2 = ((bf16[8,48,512]{2,1,0:T(8,128)(2,1)}), bf16[8,48,512]{2,1,0:T(8,128)(2,1)S(1)}, u32[]{:S(2)}, u32[]{:S(2)}) async-start(bf16[8,48,512]{2,1,0:T(8,128)(2,1)} %bitcast.23), calls=%async_computation.2 | async-start | bytes 786432 | tf_op jit(solution)/shard_map/all_to_all | solution.py:62
where the time goes:
time: 105 us; the launch traced here: 104 us
  waiting for transfers between devices  44.4 us (42%)
  local copies, waits for them, and re-layouts  19.4 us (18%)
  other arithmetic  15.3 us (15%)
  starting transfers between devices  14.6 us (14%)
  blocking collectives  8.74 us (8%)
  matrix products  1.68 us (2%)
    all_to_all x1, waiting for transfers between devices, body(): lax.all_to_all(outgoing, 'ep', split_axis=0, concat_axis=0, tiled=True)  32.3 us
    all_to_all x1, waiting for transfers between devices, body(): lax.all_to_all(summed, 'ep', split_axis=0, concat_axis=0, tiled=True)  12 us
    unnamed x1, other arithmetic  11.6 us
    all_gather x1, blocking collectives, body(): hidden_full = lax.all_gather(hidden_state, 'tp', axis=2, tiled=True)  8.74 us
    scatter x1, local copies, waits for them, and re-layouts, body(): jnp.zeros((experts * capacity, model_width), jnp.bfloat16).at[target]  6.74 us
    all_to_all x1, starting transfers between devices, body(): lax.all_to_all(outgoing, 'ep', split_axis=0, concat_axis=0, tiled=True)  6.73 us
    unnamed x19, local copies, waits for them, and re-layouts  5.36 us
    another operation x7, local copies, waits for them, and re-layouts  4.77 us
  transfers between devices with their start and end apart: 3, of which 2 were waited for; matrix products, arithmetic and copies ran while one was open for 13% of the time, Pallas kernels for 0%

commit v1 on v0

--- a/solution.py
+++ b/solution.py
@@ -1,6 +1,10 @@
+import functools
+
 import jax
 import jax.numpy as jnp
 from jax import lax
+from jax.experimental import pallas as pl
+from jax.experimental.pallas import tpu as pltpu
 from jax.sharding import PartitionSpec as P
 
 
@@ -67,9 +71,290 @@
     return combined
 
 
+MESH = pl.DeviceIdType.MESH
+F32, BF16 = jnp.float32, jnp.bfloat16
+
+
+def round_up(value, step):
+    return -(-value // step) * step
+
+
+def toggled(index, mask):
+    bit = 1
+    result = index
+    while bit <= mask:
+        if mask & bit:
+            result = result + bit * (1 - 2 * ((index // bit) % 2))
+        bit *= 2
+    return result
+
+
+def expert_kernel(
+    n_ep, n_tp, capacity, width,
+    tokens_ref, gain_ref, routes_ref, prob_ref, logits_ref, gate_ref, up_ref, down_ref,
+    out_ref,
+    normed, select, weigh, outgoing, arrived, gate_up, down_cols, hidden, result, returned,
+    send_disp, recv_disp, send_core, recv_core, send_side, recv_side, send_relay, recv_relay,
+    send_down, recv_down, send_hid, recv_hid, send_back, recv_back,
+):
+    rows, model = tokens_ref.shape
+    quarter = model // n_tp
+    fpad = gate_up.shape[1] // 2
+    n_hi = n_tp // 2
+    slots = n_ep * capacity
+    e = lax.axis_index("ep")
+    t = lax.axis_index("tp")
+    partner = t + 1 - 2 * (t % 2)
+
+    def over(index, h):
+        return (index + 2 * h) % n_tp
+
+    def back(index, h):
+        return (index + n_tp - 2 * h) % n_tp
+
+    barrier = pltpu.get_barrier_semaphore()
+    for r in range(1, n_ep):
+        pl.semaphore_signal(barrier, inc=1, device_id={"ep": toggled(e, r), "tp": t}, device_id_type=MESH)
+    for j in range(1, n_tp):
+        pl.semaphore_signal(barrier, inc=1, device_id={"ep": e, "tp": (t + j) % n_tp}, device_id_type=MESH)
+
+    routes = routes_ref[...]
+    first, second = routes[:, 0:1], routes[:, 1:2]
+    lanes = round_up(n_ep, 128)
+    expert_lane = lax.broadcasted_iota(jnp.int32, (rows, lanes), 1)
+    hit0 = (expert_lane == first).astype(F32)
+    hit1 = (expert_lane == second).astype(F32)
+    lower = (
+        lax.broadcasted_iota(jnp.int32, (rows, rows), 1) < lax.broadcasted_iota(jnp.int32, (rows, rows), 0)
+    ).astype(F32).astype(BF16)
+    earlier = jnp.dot(lower, (hit0 + hit1).astype(BF16), preferred_element_type=F32)
+    slot0 = jnp.sum(earlier * hit0, 1, keepdims=True)
+    slot1 = jnp.sum(earlier * hit1, 1, keepdims=True)
+    place0 = first * capacity + slot0.astype(jnp.int32)
+    place1 = second * capacity + slot1.astype(jnp.int32)
+    slot_lane = lax.broadcasted_iota(jnp.int32, (rows, slots), 1)
+    at0, at1 = slot_lane == place0, slot_lane == place1
+    named = at0.astype(F32) + at1.astype(F32)
+    select[...] = named.T.astype(BF16)
+
+    values = tokens_ref[...].astype(F32)
+    scale = lax.rsqrt(jnp.mean(values * values, -1, keepdims=True) + 1e-06)
+    normed[...] = (values * scale * gain_ref[...]).astype(BF16)
+
+    mine = normed[:, pl.ds(pl.multiple_of(t * quarter, quarter), quarter)]
+    packed = jnp.dot(select[...], mine, preferred_element_type=F32).astype(BF16)
+    outgoing[...] = packed.reshape(n_ep, capacity, quarter)
+
+    pl.semaphore_wait(barrier, n_ep - 1 + n_tp - 1)
+
+    def disp(r):
+        peer = toggled(e, r)
+        return pltpu.make_async_remote_copy(
+            src_ref=outgoing.at[peer], dst_ref=arrived.at[r, t], send_sem=send_disp.at[r], recv_sem=recv_disp.at[r],
+            device_id={"ep": peer, "tp": t}, device_id_type=MESH)
+
+    def core(r):
+        return pltpu.make_async_remote_copy(
+            src_ref=arrived.at[r, t], dst_ref=arrived.at[r, t], send_sem=send_core.at[r], recv_sem=recv_core.at[r],
+            device_id={"ep": e, "tp": partner}, device_id_type=MESH)
+
+    def side(r, h):
+        return pltpu.make_async_remote_copy(
+            src_ref=arrived.at[r, t], dst_ref=arrived.at[r, t], send_sem=send_side.at[r, h], recv_sem=recv_side.at[r, h],
+            device_id={"ep": e, "tp": over(t, h)}, device_id_type=MESH)
+
+    def relay(r, h):
+        origin = back(t, h)
+        return pltpu.make_async_remote_copy(
+            src_ref=arrived.at[r, origin], dst_ref=arrived.at[r, origin],
+            send_sem=send_relay.at[r, h], recv_sem=recv_relay.at[r, h],
+            device_id={"ep": e, "tp": partner}, device_id_type=MESH)
+
+    def down(j):
+        peer = (t + j) % n_tp
+        return pltpu.make_async_remote_copy(
+            src_ref=down_ref.at[:, pl.ds(pl.multiple_of(peer * quarter, quarter), quarter)],
+            dst_ref=down_cols.at[t, pl.ds(0, width)], send_sem=send_down.at[j], recv_sem=recv_down.at[j],
+            device_id={"ep": e, "tp": peer}, device_id_type=MESH)
+
+    def hid(r, j):
+        return pltpu.make_async_remote_copy(
+            src_ref=hidden.at[r, t], dst_ref=hidden.at[r, t], send_sem=send_hid.at[r, j], recv_sem=recv_hid.at[r, j],
+            device_id={"ep": e, "tp": (t + j) % n_tp}, device_id_type=MESH)
+
+    def home(r):
+        return pltpu.make_async_remote_copy(
+            src_ref=result.at[r], dst_ref=returned.at[e], send_sem=send_back.at[r], recv_sem=recv_back.at[r],
+            device_id={"ep": toggled(e, r), "tp": t}, device_id_type=MESH)
+
+    def landed(ref, sem):
+        pltpu.make_async_copy(ref, ref, sem).wait()
+
+    for r in ORDER(n_ep):
+        disp(r).start()
+    for j in range(1, n_tp):
+        down(j).start()
+
+    gate_up[...] = jnp.zeros_like(gate_up)
+    gate_up[:, 0:width] = gate_ref[...]
+    gate_up[:, fpad:fpad + width] = up_ref[...]
+    if fpad > width:
+        down_cols[:, width:fpad] = jnp.zeros((n_tp, fpad - width, quarter), BF16)
+    down_cols[t, 0:width] = down_ref[:, pl.ds(pl.multiple_of(t * quarter, quarter), quarter)]
+
+    logits = logits_ref[...]
+    logit0, logit1 = logits[:, 0:1], logits[:, 1:2]
+    top = jnp.maximum(logit0, logit1)
+    exp0, exp1 = jnp.exp(logit0 - top), jnp.exp(logit1 - top)
+    diagonal = lax.broadcasted_iota(jnp.int32, (rows, rows), 0) == lax.broadcasted_iota(jnp.int32, (rows, rows), 1)
+    prob = jnp.sum(jnp.where(diagonal, prob_ref[...], 0.0), 1, keepdims=True)
+    share = prob / (exp0 + exp1)
+    weight = jnp.where(at0, share * exp0, 0.0) + jnp.where(at1, share * exp1, 0.0)
+    high = weight.astype(BF16)
+    weigh[0] = high
+    weigh[1] = (weight - high.astype(F32)).astype(BF16)
+
+    def stage_a(r):
+        if r:
+            landed(arrived.at[r, t], recv_disp.at[r])
+            for h in range(1, n_hi):
+                side(r, h).start()
+            core(r).start()
+
+    def stage_b(r):
+        if r:
+            for h in range(1, n_hi):
+                landed(arrived.at[r, back(t, h)], recv_side.at[r, h])
+                relay(r, h).start()
+
+    def stage_c(r):
+        if r:
+            landed(arrived.at[r, partner], recv_core.at[r])
+            for h in range(1, n_hi):
+                landed(arrived.at[r, back(partner, h)], recv_relay.at[r, h])
+            acc = jnp.zeros((capacity, 2 * fpad), F32)
+            for q in range(n_tp):
+                acc = acc + jnp.dot(arrived[r, q], gate_up[q * quarter:(q + 1) * quarter], preferred_element_type=F32)
+        else:
+            own = select[pl.ds(pl.multiple_of(e * capacity, capacity), capacity)]
+            block = jnp.dot(own, normed[...], preferred_element_type=F32).astype(BF16)
+            acc = jnp.dot(block, gate_up[...], preferred_element_type=F32)
+        gate, up = acc[:, :fpad], acc[:, fpad:]
+        hidden[r, t] = (gate / (1.0 + jnp.exp(-gate)) * up).astype(BF16)
+        for j in range(1, n_tp):
+            hid(r, j).start()
+
+    def stage_d(r, first_time):
+        if first_time:
+            for j in range(1, n_tp):
+                landed(down_cols.at[(t + n_tp - j) % n_tp, pl.ds(0, width)], recv_down.at[j])
+        for j in range(1, n_tp):
+            landed(hidden.at[r, (t + n_tp - j) % n_tp], recv_hid.at[r, j])
+        acc = jnp.zeros((capacity, quarter), F32)
+        for q in range(n_tp):
+            acc = acc + jnp.dot(hidden[r, q], down_cols[q], preferred_element_type=F32)
+        if r:
+            result[r] = acc.astype(BF16)
+            home(r).start()
+        else:
+            returned[e] = acc.astype(BF16)
+
+    order = [0] + ORDER(n_ep)
+    count = len(order)
+    LAG_B, LAG_C, LAG_D = 1, 2, 3
+    for step in range(count + LAG_D):
+        if step < count:
+            stage_a(order[step])
+        if 0 <= step - LAG_B < count:
+            stage_b(order[step - LAG_B])
+        if 0 <= step - LAG_C < count:
+            stage_c(order[step - LAG_C])
+        if 0 <= step - LAG_D < count:
+            stage_d(order[step - LAG_D], step == LAG_D)
+
+    for r in ORDER(n_ep):
+        landed(returned.at[toggled(e, r)], recv_back.at[r])
+    back_rows = returned[...].reshape(slots, quarter)
+    total = jnp.dot(weigh[0], back_rows, preferred_element_type=F32)
+    total = total + jnp.dot(weigh[1], back_rows, preferred_element_type=F32)
+    out_ref[...] = total.astype(BF16)
+
+    for r in range(1, n_ep):
+        disp(r).wait_send()
+        core(r).wait_send()
+        home(r).wait_send()
+        for h in range(1, n_hi):
+            side(r, h).wait_send()
+            relay(r, h).wait_send()
+    for j in range(1, n_tp):
+        down(j).wait_send()
+        for r in range(n_ep):
+            hid(r, j).wait_send()
+
+
+def ORDER(n_ep):
+    return list(range(n_ep - 1, 0, -1))
+
+
+def fused_body(tokens, norm_gain, routes, group_prob, expert_logits, gate_weight, up_weight, down_matrix):
+    n_ep, n_tp = lax.axis_size("ep"), lax.axis_size("tp")
+    rows, model = tokens.shape
+    capacity = 3 * routes.shape[1] * rows // (2 * n_ep)
+    width = gate_weight.shape[2]
+    fpad = round_up(width, 128)
+    quarter = model // n_tp
+    n_hi = n_tp // 2
+    sem = pltpu.SemaphoreType.DMA
+    vmem = pl.BlockSpec(memory_space=pltpu.VMEM)
+    return pl.pallas_call(
+        functools.partial(expert_kernel, n_ep, n_tp, capacity, width),
+        out_shape=jax.ShapeDtypeStruct((rows, quarter), BF16),
+        in_specs=[vmem] * 8,
+        out_specs=vmem,
+        scratch_shapes=[
+            pltpu.VMEM((rows, model), BF16),
+            pltpu.VMEM((n_ep * capacity, rows), BF16),
+            pltpu.VMEM((2, rows, n_ep * capacity), BF16),
+            pltpu.VMEM((n_ep, capacity, quarter), BF16),
+            pltpu.VMEM((n_ep, n_tp, capacity, quarter), BF16),
+            pltpu.VMEM((model, 2 * fpad), BF16),
+            pltpu.VMEM((n_tp, fpad, quarter), BF16),
+            pltpu.VMEM((n_ep, n_tp, capacity, fpad), BF16),
+            pltpu.VMEM((n_ep, capacity, quarter), BF16),
+            pltpu.VMEM((n_ep, capacity, quarter), BF16),
+            sem((n_ep,)), sem((n_ep,)),
+            sem((n_ep,)), sem((n_ep,)),
+            sem((n_ep, n_hi)), sem((n_ep, n_hi)),
+            sem((n_ep, n_hi)), sem((n_ep, n_hi)),
+            sem((n_tp,)), sem((n_tp,)),
+            sem((n_ep, n_tp)), sem((n_ep, n_tp)),
+            sem((n_ep,)), sem((n_ep,)),
+        ],
+        compiler_params=pltpu.CompilerParams(collective_id=0, has_side_effects=True),
+    )(
+        tokens, norm_gain.reshape(1, model), routes, group_prob.reshape(1, rows), expert_logits,
+        gate_weight.reshape(model, width), up_weight.reshape(model, width), down_matrix.reshape(width, model),
+    )
+
+
+def fits_kernel(n_ep, n_tp, rows, experts, top, model):
+    capacity = 3 * top * rows // (2 * experts)
+    return (
+        experts == n_ep and top == 2 and n_ep & (n_ep - 1) == 0 and n_ep <= 16 and n_tp % 2 == 0
+        and capacity % 16 == 0 and rows % 128 == 0 and model % (128 * n_tp) == 0
+    )
+
+
 def solution(mesh):
+    n_ep, n_tp = mesh.shape["ep"], mesh.shape["tp"]
+
+    def chosen(*arrays):
+        rows, model = arrays[0].shape
+        fits = fits_kernel(n_ep, n_tp, rows, arrays[5].shape[0] * n_ep, arrays[2].shape[1], model)
+        return (fused_body if fits else body)(*arrays)
+
     return jax.shard_map(
-        body,
+        chosen,
         mesh=mesh,
         in_specs=(
             P("ep", None),

time: 105 us -> 47.6 us (0.45)
  waiting for transfers between devices: 44.4 us -> 0 us
  Pallas kernels: 0 us -> 40.6 us
  other arithmetic: 15.3 us -> 0 us
  starting transfers between devices: 14.6 us -> 0 us
  local copies, waits for them, and re-layouts: 19.4 us -> 6.79 us
  blocking collectives: 8.74 us -> 0 us
  matrix products: 1.68 us -> 0 us
    all_to_all x3 -> x0, waiting for transfers between devices: 44.4 us -> none  [the longest x1 32.3 us: body(): lax.all_to_all(outgoing, 'ep', split_axis=0, concat_axis=0, tiled=True)]
    pallas_call x0 -> x1, Pallas kernels: none -> 40.6 us  [fused_body(): pl.pallas_call(functools.partial(expert_kernel, n_ep, n_tp, capacity, wid...]
    all_to_all x3 -> x0, starting transfers between devices: 14.6 us -> none  [the longest x1 6.73 us: body(): lax.all_to_all(outgoing, 'ep', split_axis=0, concat_axis=0, tiled=True)]
    unnamed x1 -> x0, other arithmetic: 11.6 us -> none
    all_gather x1 -> x0, blocking collectives: 8.74 us -> none  [body(): hidden_full = lax.all_gather(hidden_state, 'tp', axis=2, tiled=True)]
    scatter x1 -> x0, local copies, waits for them, and re-layouts: 6.74 us -> none  [body(): jnp.zeros((experts * capacity, model_width), jnp.bfloat16).at[target]]
    another operation x7 -> x0, local copies, waits for them, and re-layouts: 4.77 us -> none
    reduce_sum x5 -> x0, other arithmetic: 2.8 us -> none  [the longest x1 1.36 us: body(): combined = jnp.sum(picked * weights[:, :, None], 1).astype(jnp.bfloat16)]
  transfers between devices with their start and end apart: 3 -> 0, of which waited for: 2 -> 0; matrix products, arithmetic and copies ran while one was open for 13% -> 0% of each run, Pallas kernels for 0% -> 0%
where the time goes in v1:
time: 47.6 us; the launch traced here: 47.4 us
  Pallas kernels  40.6 us (85%)
  local copies, waits for them, and re-layouts  6.79 us (14%)
    pallas_call x1, Pallas kernels, fused_body(): pl.pallas_call(functools.partial(expert_kernel, n_ep, n_tp, capacity, wid...  40.6 us
    unnamed x11, local copies, waits for them, and re-layouts  6.79 us

profile of v1, /device:TPU:0, one launch (start us, length us, event | category | flops | bytes accessed | tf_op | source)
XLA Modules:
  0.0 47.4 jit_solution(9549491903384914633)
XLA Ops:
  0.0 0.0 copy-start.1
  0.0 0.7 %copy-done.1 = s32[128,2]{0,1:T(2,128)S(1)} copy-done((s32[128,2]{0,1:T(2,128)S(1)}, s32[128,2]{0,1:T(2,128)}, u32[]{:S(2)}) %copy-start.1) | copy-done | bytes 1048
  0.7 0.0 copy-start.2
  0.7 0.7 %copy.11.routes_ref = s32[128,2]{1,0:T(8,128)} copy(s32[128,2]{0,1:T(2,128)S(1)} %copy-done.1) | data formatting | bytes 2048 | tf_op args[2]
  1.4 0.0 copy-done.2
  1.4 0.7 %copy.12.logits_ref = f32[128,2]{1,0:T(8,128)} copy(f32[128,2]{0,1:T(2,128)S(1)} %copy-done.2) | data formatting | bytes 2048 | tf_op args[4]
  2.2 0.0 copy-start
  2.2 2.0 %copy.9 = bf16[1,2048,96]{2,1,0:T(8,128)(2,1)} copy(bf16[1,2048,96]{1,2,0:T(8,128)(2,1)} %param.13) | data formatting | bytes 786432 | tf_op args[5]
  4.2 0.0 copy-done
  4.2 1.0 %copy.10 = bf16[1,2048,96]{2,1,0:T(8,128)(2,1)} copy(bf16[1,2048,96]{1,2,0:T(8,128)(2,1)S(1)} %copy-done) | data formatting | bytes 786432 | tf_op args[6]
  5.2 40.6 %shard_map.82 = bf16[128,512]{1,0:T(8,128)(2,1)} custom-call(bf16[128,2048]{1,0:T(8,128)(2,1)} %tokens_ref.1, f32[1,2048]{1,0:T(1,128)} %bitcast.8, s32[128,2]{1,0:T(8,128)} %copy.11.routes_ref, f32[1,128]{1,0:T(1,128)} %bitcast.9, f32[128,2]{1,0:T(8,128)} %copy.12.logits_ref, bf16[2048,96]{1,0:T(8,128)(2,1)} %bitcast.5, bf16[2048,96]{1,0:T(8,128)(2,1)} %bitcast.6, ...), custom_call_target="tpu_custom_call" | custom-call | tf_op jit(solution)/shard_map/pallas_call | solution.py:309
  45.8 1.6 %copy.14 = bf16[128,512]{1,0:T(8,128)(2,1)} copy(bf16[128,512]{1,0:T(8,128)(2,1)} %shard_map.82) | data formatting | bytes 262144
Async XLA Ops:
  0.0 0.7 %copy-start.1 = (s32[128,2]{0,1:T(2,128)S(1)}, s32[128,2]{0,1:T(2,128)}, u32[]{:S(2)}) copy-start(s32[128,2]{0,1:T(2,128)} %param.10) | copy-start | bytes 3076
  0.7 0.7 %copy-start.2 = (f32[128,2]{0,1:T(2,128)S(1)}, f32[128,2]{0,1:T(2,128)}, u32[]{:S(2)}) copy-start(f32[128,2]{0,1:T(2,128)} %param.12) | copy-start | bytes 3076
  2.2 2.1 %copy-start = (bf16[1,2048,96]{1,2,0:T(8,128)(2,1)S(1)}, bf16[1,2048,96]{1,2,0:T(8,128)(2,1)}, u32[]{:S(2)}) copy-start(bf16[1,2048,96]{1,2,0:T(8,128)(2,1)} %param.14) | copy-start | bytes 1179652

commit v2 on v1

--- a/solution.py
+++ b/solution.py
@@ -91,15 +91,24 @@
 
 def expert_kernel(
     n_ep, n_tp, capacity, width,
-    tokens_ref, gain_ref, routes_ref, prob_ref, logits_ref, gate_ref, up_ref, down_ref,
+    tokens_hbm, gain_hbm, routes_hbm, prob_hbm, logits_hbm, gate_ref, up_ref, down_ref,
     out_ref,
-    normed, select, weigh, outgoing, arrived, gate_up, down_cols, hidden, result, returned,
+    tokens_ref, gain_ref, routes_ref, prob_ref, logits_ref, load_sem, normed, select, weigh, outgoing, arrived, gate_up, down_cols, hidden, result, returned,
     send_disp, recv_disp, send_core, recv_core, send_side, recv_side, send_relay, recv_relay,
     send_down, recv_down, send_hid, recv_hid, send_back, recv_back,
 ):
+    loads = [
+        pltpu.make_async_copy(source, target, load_sem.at[i])
+        for i, (source, target) in enumerate((
+            (routes_hbm, routes_ref), (tokens_hbm, tokens_ref), (gain_hbm, gain_ref),
+            (prob_hbm, prob_ref), (logits_hbm, logits_ref),
+        ))
+    ]
+    for load in loads:
+        load.start()
     rows, model = tokens_ref.shape
     quarter = model // n_tp
-    fpad = gate_up.shape[1] // 2
+    fpad = gate_up.shape[0] // 2
     n_hi = n_tp // 2
     slots = n_ep * capacity
     e = lax.axis_index("ep")
@@ -118,39 +127,51 @@
     for j in range(1, n_tp):
         pl.semaphore_signal(barrier, inc=1, device_id={"ep": e, "tp": (t + j) % n_tp}, device_id_type=MESH)
 
-    routes = routes_ref[...]
-    first, second = routes[:, 0:1], routes[:, 1:2]
-    lanes = round_up(n_ep, 128)
-    expert_lane = lax.broadcasted_iota(jnp.int32, (rows, lanes), 1)
-    hit0 = (expert_lane == first).astype(F32)
-    hit1 = (expert_lane == second).astype(F32)
-    lower = (
-        lax.broadcasted_iota(jnp.int32, (rows, rows), 1) < lax.broadcasted_iota(jnp.int32, (rows, rows), 0)
+    fetch_gate = pltpu.make_async_copy(gate_ref, gate_up.at[pl.ds(0, width)], load_sem.at[5])
+    fetch_up = pltpu.make_async_copy(up_ref, gate_up.at[pl.ds(fpad, width)], load_sem.at[6])
+    fetch_down = pltpu.make_async_copy(
+        down_ref.at[:, pl.ds(pl.multiple_of(t * quarter, quarter), quarter)],
+        down_cols.at[t, pl.ds(0, width)], load_sem.at[7])
+    fetches = [fetch_gate, fetch_up, fetch_down]
+    for fetch in fetches:
+        fetch.start()
+    for load in loads:
+        load.wait()
+
+    first, second = routes_ref[0:1, :], routes_ref[1:2, :]
+    lanes = round_up(n_ep, 16)
+    expert_row = lax.broadcasted_iota(jnp.int32, (lanes, rows), 0)
+    hit0 = (expert_row == first).astype(F32)
+    hit1 = (expert_row == second).astype(F32)
+    before = (
+        lax.broadcasted_iota(jnp.int32, (rows, rows), 0) < lax.broadcasted_iota(jnp.int32, (rows, rows), 1)
     ).astype(F32).astype(BF16)
-    earlier = jnp.dot(lower, (hit0 + hit1).astype(BF16), preferred_element_type=F32)
-    slot0 = jnp.sum(earlier * hit0, 1, keepdims=True)
-    slot1 = jnp.sum(earlier * hit1, 1, keepdims=True)
+    earlier = jnp.dot((hit0 + hit1).astype(BF16), before, preferred_element_type=F32)
+    slot0 = jnp.sum(earlier * hit0, 0, keepdims=True)
+    slot1 = jnp.sum(earlier * hit1, 0, keepdims=True)
     place0 = first * capacity + slot0.astype(jnp.int32)
     place1 = second * capacity + slot1.astype(jnp.int32)
-    slot_lane = lax.broadcasted_iota(jnp.int32, (rows, slots), 1)
-    at0, at1 = slot_lane == place0, slot_lane == place1
-    named = at0.astype(F32) + at1.astype(F32)
-    select[...] = named.T.astype(BF16)
+    slot_row = lax.broadcasted_iota(jnp.int32, (slots, rows), 0)
+    at0, at1 = slot_row == place0, slot_row == place1
+    select[...] = (at0.astype(F32) + at1.astype(F32)).astype(BF16)
 
     values = tokens_ref[...].astype(F32)
     scale = lax.rsqrt(jnp.mean(values * values, -1, keepdims=True) + 1e-06)
     normed[...] = (values * scale * gain_ref[...]).astype(BF16)
 
-    mine = normed[:, pl.ds(pl.multiple_of(t * quarter, quarter), quarter)]
-    packed = jnp.dot(select[...], mine, preferred_element_type=F32).astype(BF16)
-    outgoing[...] = packed.reshape(n_ep, capacity, quarter)
+    for h in range(n_hi):
+        part = normed[:, pl.ds(pl.multiple_of(back(t, h) * quarter, quarter), quarter)]
+        packed = jnp.dot(select[...], part, preferred_element_type=F32).astype(BF16)
+        outgoing[h] = packed.reshape(n_ep, capacity, quarter)
 
     pl.semaphore_wait(barrier, n_ep - 1 + n_tp - 1)
 
-    def disp(r):
+    def disp(r, h=0):
         peer = toggled(e, r)
-        return pltpu.make_async_remote_copy(
-            src_ref=outgoing.at[peer], dst_ref=arrived.at[r, t], send_sem=send_disp.at[r], recv_sem=recv_disp.at[r],
+        origin = back(t, h)
+        return pltpu.make_async_remote_copy(
+            src_ref=outgoing.at[h, peer], dst_ref=arrived.at[r, origin],
+            send_sem=send_disp.at[r, h], recv_sem=recv_disp.at[r, h],
             device_id={"ep": peer, "tp": t}, device_id_type=MESH)
 
     def core(r):
@@ -177,9 +198,9 @@
             dst_ref=down_cols.at[t, pl.ds(0, width)], send_sem=send_down.at[j], recv_sem=recv_down.at[j],
             device_id={"ep": e, "tp": peer}, device_id_type=MESH)
 
-    def hid(r, j):
-        return pltpu.make_async_remote_copy(
-            src_ref=hidden.at[r, t], dst_ref=hidden.at[r, t], send_sem=send_hid.at[r, j], recv_sem=recv_hid.at[r, j],
+    def hid(p, j):
+        return pltpu.make_async_remote_copy(
+            src_ref=hidden.at[p, t], dst_ref=hidden.at[p, t], send_sem=send_hid.at[p, j], recv_sem=recv_hid.at[p, j],
             device_id={"ep": e, "tp": (t + j) % n_tp}, device_id_type=MESH)
 
     def home(r):
@@ -190,89 +211,105 @@
     def landed(ref, sem):
         pltpu.make_async_copy(ref, ref, sem).wait()
 
-    for r in ORDER(n_ep):
+    near = range(1, n_ep // 2)
+    far = range(max(1, n_ep // 2), n_ep)
+    for r in near:
+        for h in range(n_hi):
+            disp(r, h).start()
+    for r in far:
         disp(r).start()
     for j in range(1, n_tp):
         down(j).start()
 
-    gate_up[...] = jnp.zeros_like(gate_up)
-    gate_up[:, 0:width] = gate_ref[...]
-    gate_up[:, fpad:fpad + width] = up_ref[...]
     if fpad > width:
+        gate_up[width:fpad] = jnp.zeros((fpad - width, model), BF16)
+        gate_up[fpad + width:] = jnp.zeros((fpad - width, model), BF16)
         down_cols[:, width:fpad] = jnp.zeros((n_tp, fpad - width, quarter), BF16)
-    down_cols[t, 0:width] = down_ref[:, pl.ds(pl.multiple_of(t * quarter, quarter), quarter)]
-
-    logits = logits_ref[...]
-    logit0, logit1 = logits[:, 0:1], logits[:, 1:2]
+
+    logit0, logit1 = logits_ref[0:1, :], logits_ref[1:2, :]
     top = jnp.maximum(logit0, logit1)
     exp0, exp1 = jnp.exp(logit0 - top), jnp.exp(logit1 - top)
-    diagonal = lax.broadcasted_iota(jnp.int32, (rows, rows), 0) == lax.broadcasted_iota(jnp.int32, (rows, rows), 1)
-    prob = jnp.sum(jnp.where(diagonal, prob_ref[...], 0.0), 1, keepdims=True)
-    share = prob / (exp0 + exp1)
-    weight = jnp.where(at0, share * exp0, 0.0) + jnp.where(at1, share * exp1, 0.0)
+    share = prob_ref[...] / (exp0 + exp1)
+    weight = (jnp.where(at0, share * exp0, 0.0) + jnp.where(at1, share * exp1, 0.0)).T
     high = weight.astype(BF16)
     weigh[0] = high
     weigh[1] = (weight - high.astype(F32)).astype(BF16)
 
-    def stage_a(r):
-        if r:
-            landed(arrived.at[r, t], recv_disp.at[r])
+    def product(left, right):
+        return lax.dot_general(left, right, (((1,), (1,)), ((), ())), preferred_element_type=F32)
+
+    def take(r):
+        landed(arrived.at[r, t], recv_disp.at[r, 0])
+        if r in far:
             for h in range(1, n_hi):
                 side(r, h).start()
-            core(r).start()
-
-    def stage_b(r):
-        if r:
+        core(r).start()
+        if r in near:
             for h in range(1, n_hi):
-                landed(arrived.at[r, back(t, h)], recv_side.at[r, h])
+                landed(arrived.at[r, back(t, h)], recv_disp.at[r, h])
                 relay(r, h).start()
 
-    def stage_c(r):
-        if r:
-            landed(arrived.at[r, partner], recv_core.at[r])
-            for h in range(1, n_hi):
-                landed(arrived.at[r, back(partner, h)], recv_relay.at[r, h])
-            acc = jnp.zeros((capacity, 2 * fpad), F32)
-            for q in range(n_tp):
-                acc = acc + jnp.dot(arrived[r, q], gate_up[q * quarter:(q + 1) * quarter], preferred_element_type=F32)
-        else:
-            own = select[pl.ds(pl.multiple_of(e * capacity, capacity), capacity)]
-            block = jnp.dot(own, normed[...], preferred_element_type=F32).astype(BF16)
-            acc = jnp.dot(block, gate_up[...], preferred_element_type=F32)
+    def pass_on(r):
+        for h in range(1, n_hi):
+            landed(arrived.at[r, back(t, h)], recv_side.at[r, h])
+            relay(r, h).start()
+
+    def expand(p):
+        for r in (2 * p, 2 * p + 1):
+            if r:
+                landed(arrived.at[r, partner], recv_core.at[r])
+                for h in range(1, n_hi):
+                    landed(arrived.at[r, back(partner, h)], recv_relay.at[r, h])
+            else:
+                own = select[pl.ds(pl.multiple_of(e * capacity, capacity), capacity)]
+                for q in range(n_tp):
+                    block = jnp.dot(own, normed[:, q * quarter:(q + 1) * quarter], preferred_element_type=F32)
+                    arrived[0, q] = block.astype(BF16)
+        acc = jnp.zeros((2 * capacity, 2 * fpad), F32)
+        for q in range(n_tp):
+            block = arrived[2 * p:2 * p + 2, q].reshape(2 * capacity, quarter)
+            acc = acc + product(block, gate_up[:, q * quarter:(q + 1) * quarter])
         gate, up = acc[:, :fpad], acc[:, fpad:]
-        hidden[r, t] = (gate / (1.0 + jnp.exp(-gate)) * up).astype(BF16)
+        hidden[p, t] = (gate / (1.0 + jnp.exp(-gate)) * up).astype(BF16)
         for j in range(1, n_tp):
-            hid(r, j).start()
-
-    def stage_d(r, first_time):
-        if first_time:
+            hid(p, j).start()
+
+    def contract(p):
+        for j in range(1, n_tp):
+            landed(hidden.at[p, (t + n_tp - j) % n_tp], recv_hid.at[p, j])
+        acc = jnp.zeros((2 * capacity, quarter), F32)
+        for q in range(n_tp):
+            acc = acc + jnp.dot(hidden[p, q], down_cols[q], preferred_element_type=F32)
+        for i in range(2):
+            r = 2 * p + i
+            block = acc[i * capacity:(i + 1) * capacity].astype(BF16)
+            if r:
+                result[r] = block
+                home(r).start()
+            else:
+                returned[e] = block
+
+    for fetch in fetches:
+        fetch.wait()
+    pairs = n_ep // 2
+    todo = []
+    for p in range(pairs):
+        rounds = [r for r in (2 * p, 2 * p + 1) if r]
+        todo.append((3 * p, take, rounds))
+        todo.append((3 * p + 3, pass_on, [r for r in rounds if r in far]))
+        todo.append((3 * p + 4 if rounds[0] in far else 3 * p + 2, expand, [p]))
+        todo.append((3 * p + 8 if rounds[0] in far else 3 * p + 6, contract, [p]))
+    todo.sort(key=lambda entry: entry[0])
+    waited = False
+    for _, stage, items in todo:
+        if stage is contract and not waited:
+            waited = True
             for j in range(1, n_tp):
                 landed(down_cols.at[(t + n_tp - j) % n_tp, pl.ds(0, width)], recv_down.at[j])
-        for j in range(1, n_tp):
-            landed(hidden.at[r, (t + n_tp - j) % n_tp], recv_hid.at[r, j])
-        acc = jnp.zeros((capacity, quarter), F32)
-        for q in range(n_tp):
-            acc = acc + jnp.dot(hidden[r, q], down_cols[q], preferred_element_type=F32)
-        if r:
-            result[r] = acc.astype(BF16)
-            home(r).start()
-        else:
-            returned[e] = acc.astype(BF16)
-
-    order = [0] + ORDER(n_ep)
-    count = len(order)
-    LAG_B, LAG_C, LAG_D = 1, 2, 3
-    for step in range(count + LAG_D):
-        if step < count:
-            stage_a(order[step])
-        if 0 <= step - LAG_B < count:
-            stage_b(order[step - LAG_B])
-        if 0 <= step - LAG_C < count:
-            stage_c(order[step - LAG_C])
-        if 0 <= step - LAG_D < count:
-            stage_d(order[step - LAG_D], step == LAG_D)
-
-    for r in ORDER(n_ep):
+        for item in items:
+            stage(item)
+
+    for r in range(1, n_ep):
         landed(returned.at[toggled(e, r)], recv_back.at[r])
     back_rows = returned[...].reshape(slots, quarter)
     total = jnp.dot(weigh[0], back_rows, preferred_element_type=F32)
@@ -284,16 +321,15 @@
         core(r).wait_send()
         home(r).wait_send()
         for h in range(1, n_hi):
-            side(r, h).wait_send()
+            if r in near:
+                disp(r, h).wait_send()
+            else:
+                side(r, h).wait_send()
             relay(r, h).wait_send()
     for j in range(1, n_tp):
         down(j).wait_send()
-        for r in range(n_ep):
-            hid(r, j).wait_send()
-
-
-def ORDER(n_ep):
-    return list(range(n_ep - 1, 0, -1))
+        for p in range(pairs):
+            hid(p, j).wait_send()
 
 
 def fused_body(tokens, norm_gain, routes, group_prob, expert_logits, gate_weight, up_weight, down_matrix):
@@ -309,20 +345,26 @@
     return pl.pallas_call(
         functools.partial(expert_kernel, n_ep, n_tp, capacity, width),
         out_shape=jax.ShapeDtypeStruct((rows, quarter), BF16),
-        in_specs=[vmem] * 8,
+        in_specs=[pl.BlockSpec(memory_space=pl.ANY)] * 8,
         out_specs=vmem,
         scratch_shapes=[
             pltpu.VMEM((rows, model), BF16),
+            pltpu.VMEM((1, model), F32),
+            pltpu.VMEM((2, rows), jnp.int32),
+            pltpu.VMEM((1, rows), F32),
+            pltpu.VMEM((2, rows), F32),
+            sem((8,)),
+            pltpu.VMEM((rows, model), BF16),
             pltpu.VMEM((n_ep * capacity, rows), BF16),
             pltpu.VMEM((2, rows, n_ep * capacity), BF16),
-            pltpu.VMEM((n_ep, capacity, quarter), BF16),
+            pltpu.VMEM((n_hi, n_ep, capacity, quarter), BF16),
             pltpu.VMEM((n_ep, n_tp, capacity, quarter), BF16),
-            pltpu.VMEM((model, 2 * fpad), BF16),
+            pltpu.VMEM((2 * fpad, model), BF16),
             pltpu.VMEM((n_tp, fpad, quarter), BF16),
-            pltpu.VMEM((n_ep, n_tp, capacity, fpad), BF16),
+            pltpu.VMEM((n_ep // 2, n_tp, 2 * capacity, fpad), BF16),
             pltpu.VMEM((n_ep, capacity, quarter), BF16),
             pltpu.VMEM((n_ep, capacity, quarter), BF16),
-            sem((n_ep,)), sem((n_ep,)),
+            sem((n_ep, n_hi)), sem((n_ep, n_hi)),
             sem((n_ep,)), sem((n_ep,)),
             sem((n_ep, n_hi)), sem((n_ep, n_hi)),
             sem((n_ep, n_hi)), sem((n_ep, n_hi)),
@@ -332,8 +374,8 @@
         ],
         compiler_params=pltpu.CompilerParams(collective_id=0, has_side_effects=True),
     )(
-        tokens, norm_gain.reshape(1, model), routes, group_prob.reshape(1, rows), expert_logits,
-        gate_weight.reshape(model, width), up_weight.reshape(model, width), down_matrix.reshape(width, model),
+        tokens, norm_gain.reshape(1, model), routes.T, group_prob.reshape(1, rows), expert_logits.T,
+        gate_weight.reshape(model, width).T, up_weight.reshape(model, width).T, down_matrix.reshape(width, model),
     )
 
 

time: 47.6 us -> 39.6 us (0.83)
  local copies, waits for them, and re-layouts: 6.79 us -> 1.57 us
  Pallas kernels: 40.6 us -> 37.9 us
    unnamed x11 -> x1, local copies, waits for them, and re-layouts: 6.79 us -> 1.57 us
    pallas_call x1, Pallas kernels: 40.6 us -> 37.9 us  [fused_body(): pl.pallas_call(functools.partial(expert_kernel, n_ep, n_tp, capacity, wid...]
where the time goes in v2:
time: 39.6 us; the launch traced here: 39.4 us
  Pallas kernels  37.9 us (96%)
  local copies, waits for them, and re-layouts  1.57 us (4%)
    pallas_call x1, Pallas kernels, fused_body(): pl.pallas_call(functools.partial(expert_kernel, n_ep, n_tp, capacity, wid...  37.9 us
    unnamed x1, local copies, waits for them, and re-layouts  1.57 us

profile of v2, /device:TPU:0, one launch (start us, length us, event | category | flops | bytes accessed | tf_op | source)
XLA Modules:
  0.0 39.4 jit_solution(16172908359219256471)
XLA Ops:
  0.0 37.9 %shard_map.82 = bf16[128,512]{1,0:T(8,128)(2,1)} custom-call(bf16[128,2048]{1,0:T(8,128)(2,1)} %tokens_hbm.1, f32[1,2048]{1,0:T(1,128)} %bitcast.14, s32[2,128]{1,0:T(2,128)} %bitcast.15, f32[1,128]{1,0:T(1,128)} %bitcast.17, f32[2,128]{1,0:T(2,128)} %bitcast.16, bf16[96,2048]{1,0:T(8,128)(2,1)} %bitcast.11, bf16[96,2048]{1,0:T(8,128)(2,1)} %bitcast.12, ...), custom_call_target="tpu_custom_call" | custom-call | tf_op jit(solution)/shard_map/pallas_call | solution.py:345
  37.9 1.6 %copy.10 = bf16[128,512]{1,0:T(8,128)(2,1)} copy(bf16[128,512]{1,0:T(8,128)(2,1)} %shard_map.82) | data formatting | bytes 262144
